TPU v7x, 512 devices: a whole 4x4x16 slice. The times are simulated.
512 devices in a mesh: sp: 32 (over z, core), tp: 16 (over y, x).
Axes of the slice: x: 4, y: 4, z: 16, core: 2. Of those that a mesh axis runs over, the one named last changes fastest.
Arguments:
- residual: bfloat16 [6144, 2048], P('sp'), may hold values from -6 to 6
- query_in: bfloat16 [6144, 2048], P('sp', 'tp'), may hold values from -6 to 6
- value_in: bfloat16 [6144, 2048], P('sp', 'tp'), may hold values from -6 to 6
- forget_fwd: bfloat16 [6144, 2048], P('sp', 'tp'), may hold values from -4.5 to 4.5
- forget_bwd: bfloat16 [6144, 2048], P('sp', 'tp'), may hold values from -4.5 to 4.5
- jumps: float32 [16, 6144], P('tp', 'sp'), may hold values from -2.8 to 0
- gate_gap: float32 [2, 2048], P(None, 'tp'), may hold values from 0 to 0.1
- out_gate: bfloat16 [6144, 2048], P('sp', 'tp'), may hold values from -6 to 6
- head_gain: float32 [2048], P('tp'), may hold values from 0.1 to 1.9
- out_weight: bfloat16 [2048, 2048], P('tp'), may hold values from -0.25 to 0.25
- norm_gain: float32 [2048], replicated, may hold values from 0.1 to 1.9
- route_ids: int32 [6144, 4], P('sp'), may hold values from 0 to 31, all different within a row; in each aligned block of 192 rows (0 to 191, 192 to 383, ...) at most 36 rows name the same one
- route_weights: float32 [6144, 4], P('sp'), may hold values from 0.05 to 0.5
- w_gate: bfloat16 [32, 2048, 4096], P('sp', None, 'tp'), may hold values from -0.375 to 0.375
- w_up: bfloat16 [32, 2048, 4096], P('sp', None, 'tp'), may hold values from -0.375 to 0.375
- w_down: bfloat16 [32, 4096, 2048], P('sp', None, 'tp'), may hold values from -0.09375 to 0.09375
Outputs:
- mixed: bfloat16 [6144, 2048], P('sp', 'tp')
Inputs may be any that keep to these rules, and one draw needn't show every extreme that they name: `route_ids`: in each aligned block of 192 rows each expert is named by at most 36 rows, and by exactly 36 in some block; each row names 4 different experts.
All inputs are finite; a program needn't handle non-finite values.
Results may differ from a plain program's by a relative error of at most 0.024.
Values may be sent and summed in bfloat16 or wider, within the bound.
A program may use at most 64 MiB of HBM per device.

v0:
```python
import math

import jax
import jax.numpy as jnp
from jax import lax
from jax.sharding import Mesh
from jax.sharding import PartitionSpec as P

EXPERTS = 32
CAP = 36
SP = ("sp_0", "sp_1")


highest_precision = lax.Precision.HIGHEST
eps_norm = 1e-06
limit_value = 7.0
alpha_value = 1.702


def filled_with(x, identity):
    return jax.tree.map(
        lambda a, e: jnp.broadcast_to(jnp.asarray(e, a.dtype), a.shape), x, identity
    )


def all_in_one(x, axis):
    leaves = jax.tree.leaves(x)
    turns = sorted(range(len(leaves)), key=lambda k: -leaves[k].size)
    width = (1, *leaves[turns[0]].shape)[-1]
    lines = [
        jnp.pad(leaves[k].reshape(-1), (0, -leaves[k].size % width)).reshape(-1, width)
        for k in turns
    ]
    both, at, found = (lax.all_gather(jnp.concatenate(lines), axis), 0, {})
    for k, line in zip(turns, lines):
        section = both[:, at : at + len(line)].reshape(len(both), -1)
        found[k] = section[:, : leaves[k].size].reshape(-1, *leaves[k].shape)
        at += len(line)
    numbers = iter(range(len(leaves)))
    return jax.tree.map(lambda _: found[next(numbers)], x)


def entering(x, axes, combine, identity, reverse):
    before = start = filled_with(x, identity)
    running = x
    for axis in reversed(axes):
        length, index = (lax.axis_size(axis), lax.axis_index(axis))
        pieces = all_in_one(
            jax.tree.map(
                lambda part, kind: part.astype(kind),
                running,
                jax.tree.map(lambda a: jnp.bfloat16 if a.dtype == jnp.float32 else a.dtype, x),
            ),
            axis,
        )
        inside, running = (start, start)
        for k in reversed(range(length)) if reverse else range(length):
            passed = k > index if reverse else k < index
            running = combine(
                running, jax.tree.map(lambda part, own: part[k].astype(own.dtype), pieces, x)
            )
            inside = jax.tree.map(lambda new, old: jnp.where(passed, new, old), running, inside)
        before = combine(inside, before)
    return before


def in_blocks(x, dim, length):
    shape = x.shape
    pieces = x.reshape(*shape[:dim], length, shape[dim] // length, *shape[dim + 1 :])
    return jnp.moveaxis(pieces, dim, 0)


def sent_and_summed(x, axis, dim):
    length = lax.axis_size(axis)
    pieces = lax.all_to_all(in_blocks(x, dim, length), axis, 0, 0, tiled=True)
    return jnp.sum(pieces.astype(jnp.float32), axis=0)


def rows_for(lines, length):
    spare = -lines.shape[0] % length
    if not spare:
        return lines
    return jnp.concatenate([lines, jnp.zeros((spare, *lines.shape[1:]), lines.dtype)])


def in_order(pieces, dim):
    pieces = jnp.moveaxis(pieces, 0, dim)
    shape = pieces.shape
    return pieces.reshape(*shape[:dim], shape[dim] * shape[dim + 1], *shape[dim + 2 :])


def sent_to_all(x, axis):
    copies = jnp.broadcast_to(x, (lax.axis_size(axis), *x.shape))
    return lax.all_to_all(copies, axis, split_axis=0, concat_axis=0, tiled=True)


def gather_directly(x, axis, dim):
    return in_order(sent_to_all(x, axis), dim)


def sum_by_parts(x, axes):
    lines = x.reshape(-1, x.shape[-1])
    own = sent_and_summed(rows_for(lines, lax.axis_size(axes)), axes, 0)
    whole = gather_directly(own.astype(jnp.bfloat16), axes, 0)
    return whole[: len(lines)].reshape(x.shape).astype(jnp.float32)


def turned_blocks(pieces, axes, turns):
    inside = pieces.shape[1:]
    filled = pieces.reshape(*(lax.axis_size(a) for a in axes), *inside)
    for k in turns:
        filled = lax.all_to_all(filled, axes[k], k, k, tiled=True)
    return filled.reshape(-1, *inside)


def core_and_chips(x, groups, turns, split_dim, concat_dim):
    length = lax.axis_size(groups[0]) * lax.axis_size(groups[1])
    pieces = in_blocks(x, split_dim, length)
    return in_order(turned_blocks(pieces, groups, turns), concat_dim)


def block_pass(queries, keys_in, values, logs):
    head_rows, head_count, head_width = queries.shape
    block_size = math.gcd(head_rows, 64)
    block_count = head_rows // block_size

    def to_blocks(array):
        return array.reshape(block_count, block_size, head_count, array.shape[-1])

    q_block, k_block, v_block, log_block = (
        to_blocks(queries),
        to_blocks(keys_in),
        to_blocks(values),
        to_blocks(logs),
    )
    decay_sums = jnp.cumsum(log_block, axis=1)
    middle = decay_sums[:, block_size // 2 - 1 : block_size // 2]
    scores = jnp.einsum(
        "nthk,nshk->nhts",
        q_block * jnp.exp(decay_sums - middle),
        k_block * jnp.exp(middle - decay_sums),
        precision=highest_precision,
    )
    lower_mask = jnp.tril(jnp.ones((block_size, block_size), bool))
    within = jnp.einsum(
        "nhts,nshv->nthv", jnp.where(lower_mask, scores, 0.0), v_block, precision=highest_precision
    )
    block_end = decay_sums[:, -1]
    q_start = q_block * jnp.exp(decay_sums)
    k_end = k_block * jnp.exp(block_end[:, None] - decay_sums)

    def advance(current_state, block_items):
        query_segment, key_segment, value_segment, decay_part = block_items
        state_readout = jnp.einsum(
            "qwe,wei->qwi", query_segment, current_state, precision=highest_precision
        )
        current_state = current_state * jnp.exp(decay_part)[:, :, None] + jnp.einsum(
            "foj,fox->ojx", key_segment, value_segment, precision=highest_precision
        )
        return (current_state, state_readout)

    zero_state = jnp.zeros((head_count, head_width, values.shape[-1]), jnp.float32)
    final_state, across = lax.scan(advance, zero_state, (q_start, k_end, v_block, block_end))
    return ((within + across).reshape(head_rows, head_count, -1), final_state)


def combine_states(first_part, second_part):
    return (
        first_part[0] * second_part[0],
        second_part[0][:, :, None] * first_part[1] + second_part[1],
    )


def carried(queries, logs, running_state):
    decayed_state = queries * jnp.exp(jnp.cumsum(logs, axis=0))
    return jnp.einsum("una,nae->une", decayed_state, running_state, precision=highest_precision)


def shards(
    residual,
    query_in,
    value_in,
    forget_fwd,
    forget_bwd,
    jumps,
    gate_gap,
    out_gate,
    head_gain,
    out_weight,
    norm_gain,
    route_ids,
    route_weights,
    w_gate,
    w_up,
    w_down,
):
    head_rows, local_width = query_in.shape
    head_count = jumps.shape[0]
    head_width = local_width // head_count

    def by_head(array):
        return array.astype(jnp.float32).reshape(head_rows, head_count, head_width)

    queries = jax.nn.silu(by_head(query_in))
    values = by_head(value_in)
    jump_rows = jnp.transpose(jumps)[:, :, None]

    def gate_terms(forget_in, gap):
        key_share = gap.reshape(head_count, head_width) * jax.nn.sigmoid(-by_head(forget_in))
        return (key_share, jnp.log1p(-key_share) + jump_rows)

    keys_fwd, logs_fwd = gate_terms(forget_fwd, gate_gap[0])
    keys_bwd, logs_bwd = gate_terms(forget_bwd, gate_gap[1])
    ones_part = jnp.ones((head_count, head_width), jnp.float32)
    zero_part = jnp.zeros((head_count, head_width, head_width), jnp.float32)
    local_fwd, final_fwd = block_pass(queries, keys_fwd, values, logs_fwd)
    summary_fwd = (jnp.exp(jnp.sum(logs_fwd, axis=0)), final_fwd)
    carry_fwd = entering(summary_fwd, SP, combine_states, (ones_part, zero_part), False)[1]
    flip_queries = jnp.flip(queries, 0)
    flip_logs = jnp.flip(logs_bwd, 0)
    local_bwd, final_bwd = block_pass(
        flip_queries, jnp.flip(keys_bwd, 0), jnp.flip(values, 0), flip_logs
    )
    summary_bwd = (jnp.exp(jnp.sum(logs_bwd, axis=0)), final_bwd)
    carry_bwd = entering(summary_bwd, SP, combine_states, (ones_part, zero_part), True)[1]
    forward_out = local_fwd + carried(queries, logs_fwd, carry_fwd)
    backward_out = jnp.flip(local_bwd + carried(flip_queries, flip_logs, carry_bwd), 0)
    mixed_heads = forward_out + backward_out
    mean_square = jnp.mean(mixed_heads * mixed_heads, axis=-1, keepdims=True)
    normed = (mixed_heads * lax.rsqrt(mean_square + eps_norm)).reshape(head_rows, local_width)
    gated = (normed * head_gain * jax.nn.silu(out_gate.astype(jnp.float32))).astype(jnp.bfloat16)
    head_terms = jnp.dot(gated, out_weight, preferred_element_type=jnp.float32)
    summed = sum_by_parts(head_terms.astype(jnp.bfloat16), "tp")
    stream = (residual.astype(jnp.float32) + summed).astype(jnp.bfloat16)
    stream_f = stream.astype(jnp.float32)
    row_scale = lax.rsqrt(jnp.mean(stream_f * stream_f, axis=-1, keepdims=True) + eps_norm)
    normed_rows = (stream_f * row_scale * norm_gain).astype(jnp.bfloat16)
    top_count = route_ids.shape[1]
    flat_ids = route_ids.reshape(-1)
    one_hot = (flat_ids[:, None] == jnp.arange(EXPERTS, dtype=jnp.int32)[None, :]).astype(jnp.int32)
    slot_rank = jnp.sum((jnp.cumsum(one_hot, axis=0) - 1) * one_hot, axis=1)
    slot_index = flat_ids * CAP + slot_rank
    owner_rows = jnp.arange(head_rows * top_count, dtype=jnp.int32) // top_count
    slot_rows = jnp.full((EXPERTS * CAP,), head_rows, jnp.int32).at[slot_index].set(owner_rows)
    padded_rows = jnp.concatenate(
        [normed_rows, jnp.zeros((1, normed_rows.shape[1]), jnp.bfloat16)], axis=0
    )
    tp_index = lax.axis_index("tp")
    part_width = w_down.shape[2]
    column_rows = lax.dynamic_slice_in_dim(padded_rows, tp_index * part_width, part_width, 1)
    buffer = column_rows[slot_rows].reshape(EXPERTS, CAP, part_width)
    arrived = lax.all_to_all(buffer, SP, split_axis=0, concat_axis=1, tiled=True)
    piece = lax.all_gather(arrived, "tp", axis=2, tiled=True)
    gate_sum = jnp.einsum("esd,edf->esf", piece, w_gate, preferred_element_type=jnp.float32)
    up_sum = jnp.einsum("esd,edf->esf", piece, w_up, preferred_element_type=jnp.float32)
    gate_sum = jnp.minimum(gate_sum, limit_value)
    up_sum = jnp.clip(up_sum, -limit_value, limit_value)
    active = (gate_sum * jax.nn.sigmoid(alpha_value * gate_sum) * (up_sum + 1.0)).astype(
        jnp.bfloat16
    )
    produced = jnp.einsum(
        "esf,efd->esd",
        lax.all_gather(active, "tp", axis=2, tiled=True),
        w_down,
        preferred_element_type=jnp.float32,
    ).astype(jnp.bfloat16)
    returned = core_and_chips(produced, ("sp_0", "sp_1"), (1, 0), 1, 0)
    picked = returned.reshape(EXPERTS * CAP, part_width)[slot_index].astype(jnp.float32)
    picked = picked.reshape(head_rows, top_count, part_width)
    moe_out = jnp.sum(picked * route_weights[:, :, None], axis=1)
    own_columns = lax.dynamic_slice_in_dim(stream_f, tp_index * part_width, part_width, 1)
    return (own_columns + moe_out).astype(jnp.bfloat16)


def solution(mesh):
    finer = Mesh(mesh.devices.reshape(16, 2, mesh.shape["tp"]), ("sp_0", "sp_1", "tp"))
    return jax.shard_map(
        shards,
        mesh=finer,
        in_specs=(
            P(SP, None),
            P(SP, "tp"),
            P(SP, "tp"),
            P(SP, "tp"),
            P(SP, "tp"),
            P("tp", SP),
            P(None, "tp"),
            P(SP, "tp"),
            P("tp"),
            P("tp", None),
            P(),
            P(SP, None),
            P(SP, None),
            P(SP, None, "tp"),
            P(SP, None, "tp"),
            P(SP, None, "tp"),
        ),
        out_specs=P(SP, "tp"),
        check_vma=False,
    )
```

profile of v0, /device:TPU:1, one launch (start us, length us, event | category | flops | bytes accessed | tf_op | source)
XLA Modules:
  0.0 393.2 jit_solution(2136767596949991621)
XLA Ops:
  7.3 1.0 fusion.388
  10.9 1.7 while.26
  12.6 8.3 %all-gather.5 = bf16[2,129,128]{2,1,0:T(8,128)(2,1)S(1)} all-gather(bf16[1,129,128]{2,1,0:T(8,128)(2,1)S(1)} %maximum_bitcast_fusion), channel_id=2, replica_groups=mesh['sp_0'=16,'sp_1'=2,'tp'=16] {'sp_1'}, dimensions={0}, use_global_device_ids=true | all-gather | bytes 99072 | tf_op jit(solution)/shard_map/all_gather | solution.py:34
  21.7 26.3 %all-gather.6 = bf16[16,129,128]{2,1,0:T(8,128)(2,1)S(1)} all-gather(bf16[1,129,128]{2,1,0:T(8,128)(2,1)S(1)} %maximum_bitcast_fusion.1), channel_id=3, replica_groups=mesh['sp_0'=16,'sp_1'=2,'tp'=16] {'sp_0'}, dimensions={0}, use_global_device_ids=true | all-gather | bytes 561408 | tf_op jit(solution)/shard_map/all_gather | solution.py:34
  51.0 1.7 while.27
  52.8 8.6 %all-gather.7 = bf16[2,129,128]{2,1,0:T(8,128)(2,1)S(1)} all-gather(bf16[1,129,128]{2,1,0:T(8,128)(2,1)S(1)} %maximum_bitcast_fusion.2), channel_id=4, replica_groups=mesh['sp_0'=16,'sp_1'=2,'tp'=16] {'sp_1'}, dimensions={0}, use_global_device_ids=true | all-gather | bytes 99072 | tf_op jit(solution)/shard_map/all_gather | solution.py:34
  62.1 22.3 %all-gather.8 = bf16[16,129,128]{2,1,0:T(8,128)(2,1)S(1)} all-gather(bf16[1,129,128]{2,1,0:T(8,128)(2,1)S(1)} %maximum_bitcast_fusion.3), channel_id=5, replica_groups=mesh['sp_0'=16,'sp_1'=2,'tp'=16] {'sp_0'}, dimensions={0}, use_global_device_ids=true | all-gather | bytes 561408 | tf_op jit(solution)/shard_map/all_gather | solution.py:34
  86.4 1.1 fusion.41
  87.7 1.5 fusion.39
  90.3 1.6 multiply_reduce_fusion.1
  92.3 1.2 reshape.1657
  93.5 6.8 %all-to-all-start = ((bf16[16,12,2048]{2,1,0:T(8,128)(2,1)}), bf16[16,12,2048]{2,1,0:T(8,128)(2,1)S(1)}, u32[]{:S(2)}, u32[]{:S(2)}) async-start(bf16[16,12,2048]{2,1,0:T(8,128)(2,1)} %reshape.1657), calls=%async_computation | async-start | bytes 2097152 | tf_op jit(solution)/shard_map/all_to_all | solution.py:75
  100.5 1.7 reduce-window.26
  102.3 10.2 %all-to-all-done = bf16[16,12,2048]{2,1,0:T(8,128)(2,1)S(1)} async-done(((bf16[16,12,2048]{2,1,0:T(8,128)(2,1)}), bf16[16,12,2048]{2,1,0:T(8,128)(2,1)S(1)}, u32[]{:S(2)}, u32[]{:S(2)}) %all-to-all-start) | async-done | bytes 786464 | tf_op jit(solution)/shard_map/all_to_all | solution.py:75
  112.7 1.1 broadcast_in_dim.35
  113.8 3.7 all-to-all-start.1
  118.3 3.4 scatter_custom_fusion
  121.7 7.9 %all-to-all-done.1 = bf16[16,12,2048]{2,1,0:T(8,128)(2,1)S(1)} async-done(((bf16[16,12,2048]{2,1,0:T(8,128)(2,1)}), bf16[16,12,2048]{2,1,0:T(8,128)(2,1)S(1)}, u32[]{:S(2)}, u32[]{:S(2)}) %all-to-all-start.1) | async-done | bytes 786464 | tf_op jit(solution)/shard_map/all_to_all | solution.py:94
  129.6 1.3 reshape.1699
  130.9 1.7 multiply_reduce_fusion
  132.9 2.9 gather_fusion
  135.9 42.3 %all_to_all.32 = bf16[32,36,128]{2,1,0:T(8,128)(2,1)S(1)} all-to-all(bf16[32,36,128]{2,1,0:T(8,128)(2,1)S(1)} %reshape.1659), channel_id=1, replica_groups=mesh['sp_0'=16,'sp_1'=2,'tp'=16] {'sp_0','sp_1'}, dimensions={0} | all-to-all | bytes 589824 | tf_op jit(solution)/shard_map/all_to_all | solution.py:252
  179.2 60.6 %all-gather.12.cloned.1.call-done = bf16[1,1152,2048]{2,1,0:T(8,128)(2,1)} async-done(((bf16[1,1152,128]{2,1,0:T(8,128)(2,1)}), bf16[1,1152,2048]{2,1,0:T(8,128)(2,1)}) %all-gather.12.cloned.1.call-update) | async-done | bytes 4718608 | tf_op jit(solution)/shard_map/all_gather | solution.py:253
  239.8 3.9 fusion.25
  243.9 2.4 fusion.34
  246.3 97.4 %all-gather.14.cloned.1.call-done = bf16[1152,4096]{1,0:T(8,128)(2,1)} async-done(((bf16[1152,256]{1,0:T(8,128)(2,1)}), bf16[1152,4096]{1,0:T(8,128)(2,1)}) %all-gather.14.cloned.1.call-update) | async-done | bytes 9437200 | tf_op jit(solution)/shard_map/all_gather | solution.py:263
  343.7 6.5 %convolution_convert_fusion.1 = bf16[1152,128]{1,0:T(8,128)(2,1)S(1)} fusion(bf16[1152,4096]{1,0:T(8,128)(2,1)} %all-gather.14.cloned.1.call-done, bf16[1,4096,128]{2,1,0:T(8,128)(2,1)} %param.35), kind=kOutput, calls=%fused_computation.43 | convolution fusion | flops 1208107008 | bytes 10780672 | tf_op jit(solution)/shard_map/esf,efd->esd/dot_general | solution.py:261
  350.4 5.6 %all_to_all.33 = bf16[16,2,1,36,128]{4,0,3,2,1:T(8,128)(2,1)S(1)} all-to-all(bf16[16,2,1,36,128]{4,0,3,2,1:T(8,128)(2,1)S(1)} %copy.63), channel_id=1, replica_groups=mesh['sp_0'=16,'sp_1'=2,'tp'=16] {'sp_1'}, dimensions={1} | all-to-all | bytes 589824 | tf_op jit(solution)/shard_map/all_to_all | solution.py:112
  356.1 1.0 copy.64
  357.1 12.0 %all-to-all-start.4 = ((bf16[16,2,1,36,128]{4,1,3,2,0:T(2,128)(2,1)}), bf16[16,2,1,36,128]{4,1,3,2,0:T(2,128)(2,1)S(1)}, u32[]{:S(2)}, u32[]{:S(2)}) async-start(bf16[16,2,1,36,128]{4,1,3,2,0:T(2,128)(2,1)} %copy.64), calls=%async_computation.4 | async-start | bytes 589824 | tf_op jit(solution)/shard_map/all_to_all | solution.py:112
  369.2 14.2 %all-to-all-done.4 = bf16[16,2,1,36,128]{4,1,3,2,0:T(2,128)(2,1)S(1)} async-done(((bf16[16,2,1,36,128]{4,1,3,2,0:T(2,128)(2,1)}), bf16[16,2,1,36,128]{4,1,3,2,0:T(2,128)(2,1)S(1)}, u32[]{:S(2)}, u32[]{:S(2)}) %all-to-all-start.4) | async-done | bytes 294944 | tf_op jit(solution)/shard_map/all_to_all | solution.py:112
  383.5 1.9 gather_fusion.1
  (204 shorter events, 17.9 us)
Async XLA Ops:
  6.5 233.3 %copy-start = (bf16[1,2048,256]{2,1,0:T(8,128)(2,1)S(1)}, bf16[1,2048,256]{2,1,0:T(8,128)(2,1)}, u32[]{:S(2)}) copy-start(bf16[1,2048,256]{2,1,0:T(8,128)(2,1)} %param.33) | copy-start | bytes 3145732
  10.9 38.5 %copy-start.3 = (bf16[192,128]{1,0:T(8,128)(2,1)S(1)}, bf16[192,128]{1,0:T(8,128)(2,1)}, u32[]{:S(2)}) copy-start(bf16[192,128]{1,0:T(8,128)(2,1)} %param.22) | copy-start | bytes 147460
  12.6 36.1 %copy-start.4 = (f32[3,64,1,128]{3,1,2,0:T(8,128)}, f32[3,64,1,128]{3,1,2,0:T(8,128)S(1)}, u32[]{:S(2)}) copy-start(f32[3,64,1,128]{3,1,2,0:T(8,128)S(1)} %get-tuple-element.81) | copy-start | bytes 294916
  21.0 28.8 %copy-start.7 = (bf16[2,129,128]{2,1,0:T(8,128)(2,1)}, bf16[2,129,128]{2,1,0:T(8,128)(2,1)S(1)}, u32[]{:S(2)}) copy-start(bf16[2,129,128]{2,1,0:T(8,128)(2,1)S(1)} %all-gather.5) | copy-start | bytes 198148
  21.0 28.9 %copy-start.19 = (f32[128]{0:T(128)}, f32[128]{0:T(128)S(1)}, u32[]{:S(2)}) copy-start(f32[128]{0:T(128)S(1)} %fusion.382) | copy-start | bytes 1540
  21.6 28.2 %copy-start.16 = (f32[128]{0:T(128)}, f32[128]{0:T(128)S(1)}, u32[]{:S(2)}) copy-start(f32[128]{0:T(128)S(1)} %get-tuple-element.212) | copy-start | bytes 1540
  52.7 9.4 %copy-start.6 = (f32[3,64,1,128]{3,1,2,0:T(8,128)}, f32[3,64,1,128]{3,1,2,0:T(8,128)S(1)}, u32[]{:S(2)}) copy-start(f32[3,64,1,128]{3,1,2,0:T(8,128)S(1)} %get-tuple-element.83) | copy-start | bytes 294916
  52.8 33.3 %copy-start.12 = (f32[3,128]{1,0:T(4,128)S(1)}, f32[3,128]{1,0:T(4,128)}, u32[]{:S(2)}) copy-start(f32[3,128]{1,0:T(4,128)} %get-tuple-element.225) | copy-start | bytes 4612
  61.4 24.2 %copy-start.8 = (bf16[2,129,128]{2,1,0:T(8,128)(2,1)}, bf16[2,129,128]{2,1,0:T(8,128)(2,1)S(1)}, u32[]{:S(2)}) copy-start(bf16[2,129,128]{2,1,0:T(8,128)(2,1)S(1)} %all-gather.7) | copy-start | bytes 198148
  86.4 3.2 copy-start.11
  87.5 2.6 copy-start.10
  87.5 2.6 copy-start.17
  87.5 2.6 copy-start.20
  87.5 2.6 copy-start.21
  87.6 2.6 copy-start.22
  87.6 2.6 copy-start.23
  87.6 2.6 copy-start.24
  87.6 2.6 copy-start.25
  87.6 2.6 copy-start.26
  87.6 2.6 copy-start.27
  87.6 2.6 copy-start.28
  87.6 2.6 copy-start.29
  92.3 7.9 %copy-start.13 = (s32[192,4]{0,1:T(4,128)S(1)}, s32[192,4]{0,1:T(4,128)}, u32[]{:S(2)}) copy-start(s32[192,4]{0,1:T(4,128)} %param.31) | copy-start | bytes 9220
  93.5 19.0 %all-to-all-start = ((bf16[16,12,2048]{2,1,0:T(8,128)(2,1)}), bf16[16,12,2048]{2,1,0:T(8,128)(2,1)S(1)}, u32[]{:S(2)}, u32[]{:S(2)}) async-start(bf16[16,12,2048]{2,1,0:T(8,128)(2,1)} %reshape.1657), calls=%async_computation | async-start | bytes 2097152 | tf_op jit(solution)/shard_map/all_to_all | solution.py:75
  113.8 15.8 %all-to-all-start.1 = ((bf16[16,12,2048]{2,1,0:T(8,128)(2,1)}), bf16[16,12,2048]{2,1,0:T(8,128)(2,1)S(1)}, u32[]{:S(2)}, u32[]{:S(2)}) async-start(bf16[16,12,2048]{2,1,0:T(8,128)(2,1)} %broadcast_in_dim.35), calls=%async_computation.1 | async-start | bytes 2097152 | tf_op jit(solution)/shard_map/all_to_all | solution.py:94
  117.4 122.4 %all-gather.12.cloned.1.call-start = ((), (), s32[]{:S(2)}) async-start(), calls=%async_computation.5 | async-start | bytes 5013504 | tf_op jit(solution)/shard_map/all_gather | solution.py:253
  117.7 13.2 %copy-start.1 = (bf16[192,2048]{1,0:T(8,128)(2,1)S(1)}, bf16[192,2048]{1,0:T(8,128)(2,1)}, u32[]{:S(2)}) copy-start(bf16[192,2048]{1,0:T(8,128)(2,1)} %param.20) | copy-start | bytes 2359300
  179.0 164.7 %all-gather.14.cloned.1.call-start = ((), (), s32[]{:S(2)}) async-start(), calls=%async_computation.6 | async-start | bytes 10027008 | tf_op jit(solution)/shard_map/all_gather | solution.py:263
  239.8 3.9 copy-start.37
  239.8 4.1 %copy-start.38 = (bf16[1,2048,256]{2,1,0:T(8,128)(2,1)S(1)}, bf16[1,2048,256]{2,1,0:T(8,128)(2,1)}, u32[]{:S(2)}) copy-start(bf16[1,2048,256]{2,1,0:T(8,128)(2,1)} %param.34) | copy-start | bytes 3145732
  350.3 18.8 %copy-start.15 = (f32[192,4]{0,1:T(4,128)S(1)}, f32[192,4]{0,1:T(4,128)}, u32[]{:S(2)}) copy-start(f32[192,4]{0,1:T(4,128)} %param.32) | copy-start | bytes 9220
  357.1 26.3 %all-to-all-start.4 = ((bf16[16,2,1,36,128]{4,1,3,2,0:T(2,128)(2,1)}), bf16[16,2,1,36,128]{4,1,3,2,0:T(2,128)(2,1)S(1)}, u32[]{:S(2)}, u32[]{:S(2)}) async-start(bf16[16,2,1,36,128]{4,1,3,2,0:T(2,128)(2,1)} %copy.64), calls=%async_computation.4 | async-start | bytes 589824 | tf_op jit(solution)/shard_map/all_to_all | solution.py:112
  (13 other events, 31.5 us)
Sparse Core Ops, SparseCore 0:
  179.1 60.6 all-gather.11
  246.5 97.2 all-gather.13
where the time goes:
time: 398 us; the launch traced here: 393 us
  waiting for transfers between devices  190 us (48%)
  blocking collectives  113 us (28%)
  starting transfers between devices  22.7 us (6%)
  matrix products  21.1 us (5%)
  local copies, waits for them, and re-layouts  18.4 us (5%)
  between operations  14.5 us (4%)
  other arithmetic  12.4 us (3%)
    all_gather x1, waiting for transfers between devices, shards(): lax.all_gather(active, 'tp', axis=2, tiled=True)  97.4 us
    all_gather x4, blocking collectives, all_in_one(): both, at, found = (lax.all_gather(jnp.concatenate(lines), axis), 0, {})  65.5 us
    all_gather x1, waiting for transfers between devices, shards(): piece = lax.all_gather(arrived, 'tp', axis=2, tiled=True)  60.6 us
    all_to_all x1, blocking collectives, shards(): lax.all_to_all(buffer, SP, split_axis=0, concat_axis=1, tiled=True)  42.3 us
    all_to_all x1, waiting for transfers between devices, turned_blocks(): filled = lax.all_to_all(filled, axes[k], k, k, tiled=True)  14.2 us
    all_to_all x1, starting transfers between devices, turned_blocks(): filled = lax.all_to_all(filled, axes[k], k, k, tiled=True)  12 us
    all_to_all x1, waiting for transfers between devices, sent_and_summed(): pieces = lax.all_to_all(in_blocks(x, dim, length), axis, 0, 0, tiled=True)  10.2 us
  transfers between devices with their start and end apart: 5, of which 5 were waited for; matrix products, arithmetic and copies ran while one was open for 2% of the time, Pallas kernels for 0%

commit v1 on v0

v1 whole, which is shorter than its diff:
```python
import jax
import jax.numpy as jnp
from jax import lax
from jax.experimental import pallas as pl
from jax.experimental.pallas import tpu as pltpu
from jax.sharding import PartitionSpec as P

MESH = pl.DeviceIdType.MESH
HIGH = lax.Precision.HIGHEST
F32 = jnp.float32
BF16 = jnp.bfloat16
NSP = 32
NTP = 16
T = 192
W = 128
CAP = 36
PAD = 48
ROWS = NSP * CAP
SLOTS = NSP * PAD
TILE = 288
EPS = 1e-06
LIMIT = 7.0
ALPHA = 1.702


def iota(shape, dim):
    return lax.broadcasted_iota(jnp.int32, shape, dim)


def nn(a, b, precision=None):
    return jnp.dot(a, b, preferred_element_type=F32, precision=precision)


def nt(a, b, precision=None):
    return lax.dot_general(a, b, (((1,), (1,)), ((), ())), preferred_element_type=F32, precision=precision)


def tn(a, b, precision=None):
    return lax.dot_general(a, b, (((0,), (0,)), ((), ())), preferred_element_type=F32, precision=precision)


def onehot(mask):
    return jnp.where(mask, 1.0, 0.0).astype(BF16)


def split(a):
    high = a.astype(BF16)
    return high, (a - high.astype(F32)).astype(BF16)


def remote(src, dst, send, recv, device):
    return pltpu.make_async_remote_copy(
        src_ref=src, dst_ref=dst, send_sem=send, recv_sem=recv, device_id=device, device_id_type=MESH
    )


class Exchange:
    def __init__(self, axis, size, source, target, send, recv):
        self.axis, self.size, self.source, self.target = axis, size, source, target
        self.send, self.recv = send, recv
        self.me = lax.axis_index(axis)

    def copy(self, d, to, slot):
        return remote(
            self.source(to), self.target(slot), self.send.at[d], self.recv.at[d], {self.axis: to}
        )

    def start(self):
        @pl.loop(1, self.size)
        def _(d):
            to = lax.rem(self.me + d, self.size)
            self.copy(d, to, self.me).start()

    def wait(self):
        @pl.loop(1, self.size)
        def _(d):
            origin = lax.rem(self.me - d + self.size, self.size)
            self.copy(d, origin, origin).wait()


class Torus:
    def __init__(self):
        t = lax.axis_index("tp")
        self.y, self.x = t // 4, lax.rem(t, 4)

    def index(self, along_x):
        return self.x if along_x else self.y

    def device(self, along_x, j):
        return {"tp": self.y * 4 + j if along_x else j * 4 + self.x}


def near(i):
    return lax.rem(i + 1, 4), lax.rem(i + 3, 4), lax.rem(i + 2, 4)


class Gather:
    def __init__(self, torus, ref, rows, base, send, recv, number):
        self.t, self.ref, self.rows, self.base = torus, ref, rows, base
        self.send, self.recv, self.number = send, recv, number

    def view(self, half, stage, j, q):
        piece = self.rows // 4
        rows = pl.ds(self.base + half * (self.rows // 2) + q * piece, piece)
        if (half == 0) == (stage == 0):
            return self.ref.at[self.t.y, j, rows] if stage == 0 else self.ref.at[:, j, rows]
        return self.ref.at[j, self.t.x, rows] if stage == 0 else self.ref.at[j, :, rows]

    def copy(self, half, stage, k, arriving=False):
        along = (half == 0) == (stage == 0)
        i = self.t.index(along)
        p, m, f = near(i)
        up = k < 3
        to = p if up else m
        q = (0, 1, 0, 1, 0, 1)[k]
        if arriving:
            j = (m, m, f, p, p, f)[k]
        else:
            j = (i, i, m, i, i, p)[k]
        ref = self.view(half, stage, j, q)
        n = self.number * 24 + half * 12 + stage * 6 + k
        return remote(ref, ref, self.send.at[n], self.recv.at[n], self.t.device(along, to))

    def begin(self, half, stage):
        for k in (0, 3, 1, 4):
            self.copy(half, stage, k).start()

    def relay(self, half, stage):
        for k, then in ((0, 2), (3, 5)):
            self.copy(half, stage, k, True).wait_recv()
            self.copy(half, stage, then).start()

    def end(self, half, stage):
        for k in (1, 4, 2, 5):
            self.copy(half, stage, k, True).wait_recv()

    def drain(self):
        for half in range(2):
            for stage in range(2):
                for k in range(6):
                    self.copy(half, stage, k).wait_send()

    def run(self):
        for stage in range(2):
            for half in range(2):
                self.begin(half, stage)
            for half in range(2):
                self.relay(half, stage)
            for half in range(2):
                self.end(half, stage)


class Reduce:
    def __init__(self, torus, ref, rows, base, wide, narrow, send, recv, number):
        self.t, self.ref, self.rows, self.base = torus, ref, rows, base
        self.wide, self.narrow, self.send, self.recv, self.number = wide, narrow, send, recv, number

    def along(self, half, stage):
        return (half == 0) != (stage == 0)

    def view(self, half, stage, j, q):
        piece = self.rows // 4
        rows = pl.ds(self.base + half * (self.rows // 2) + q * piece, piece)
        if self.along(half, stage):
            return self.ref.at[self.t.y, j, rows] if stage == 1 else self.ref.at[:, j, rows]
        return self.ref.at[j, self.t.x, rows] if stage == 1 else self.ref.at[j, :, rows]

    def slot(self, half, stage, k):
        n = (self.number * 2 + half) * 6 + k
        return self.wide.at[n] if stage == 0 else self.narrow.at[n]

    def copy(self, half, stage, k):
        along = self.along(half, stage)
        i = self.t.index(along)
        p, m, f = near(i)
        to = p if k < 3 else m
        q = (0, 1, 0, 1, 0, 1)[k]
        j = (f, p, p, f, m, m)[k]
        n = self.number * 24 + half * 12 + stage * 6 + k
        return remote(
            self.view(half, stage, j, q),
            self.slot(half, stage, k),
            self.send.at[n],
            self.recv.at[n],
            self.t.device(along, to),
        )

    def add(self, half, stage, j, q, ks):
        own = self.view(half, stage, j, q)
        refs = [self.slot(half, stage, k) for k in ks]
        if stage == 0:
            @pl.loop(0, 4)
            def _(a):
                total = own[a].astype(F32)
                for ref in refs:
                    total = total + ref[a].astype(F32)
                own[a] = total.astype(BF16)
        else:
            total = own[...].astype(F32)
            for ref in refs:
                total = total + ref[...].astype(F32)
            own[...] = total.astype(BF16)

    def begin(self, half, stage):
        for k in (0, 3, 1, 4):
            self.copy(half, stage, k).start()

    def relay(self, half, stage):
        p, m, f = near(self.t.index(self.along(half, stage)))
        self.copy(half, stage, 0).wait_recv()
        self.add(half, stage, p, 0, (0,))
        self.copy(half, stage, 2).start()
        self.copy(half, stage, 3).wait_recv()
        self.add(half, stage, m, 1, (3,))
        self.copy(half, stage, 5).start()

    def end(self, half, stage):
        i = self.t.index(self.along(half, stage))
        for q, ks in ((0, (2, 4)), (1, (1, 5))):
            for k in ks:
                self.copy(half, stage, k).wait_recv()
            self.add(half, stage, i, q, ks)

    def drain(self):
        for half in range(2):
            for stage in range(2):
                for k in range(6):
                    self.copy(half, stage, k).wait_send()

    def run(self):
        for stage in range(2):
            for half in range(2):
                self.begin(half, stage)
            for half in range(2):
                self.relay(half, stage)
            for half in range(2):
                self.end(half, stage)


def layer(
    residual, query_in, value_in, forget_fwd, forget_bwd, jumps, gate_gap, out_gate, head_gain,
    out_weight, norm_gain, route_ids, route_weights, w_gate, w_up, w_down,
    mixed,
    wg, wu, wd, wo, res, states, got, scanned, answers, carries,
    gat, disp, comb, sent, came, rows, xs, act, part, wide, narrow, outs, back,
    local, zsend, zrecv, tsend, trecv, gsend, grecv, rsend, rrecv,
):
    sp, tp = lax.axis_index("sp"), lax.axis_index("tp")
    torus = Torus()
    y, x = torus.y, torus.x

    barrier = pltpu.get_barrier_semaphore()

    @pl.loop(1, NSP)
    def _(d):
        pl.semaphore_signal(barrier, 1, device_id={"sp": lax.rem(sp + d, NSP)}, device_id_type=MESH)

    @pl.loop(1, NTP)
    def _(d):
        pl.semaphore_signal(barrier, 1, device_id={"tp": lax.rem(tp + d, NTP)}, device_id_type=MESH)

    mine_t = pl.ds(pl.multiple_of(tp * W, W), W)
    own = [
        pltpu.make_async_copy(residual.at[:, mine_t], res, local.at[0]),
        pltpu.make_async_copy(out_weight.at[:, mine_t], wo.at[tp], local.at[1]),
        pltpu.make_async_copy(w_gate.at[0], wg, local.at[2]),
        pltpu.make_async_copy(w_up.at[0], wu, local.at[3]),
        pltpu.make_async_copy(
            w_down.at[0, pl.ds(pl.multiple_of(tp * 256, 256), 256)], wd.at[:, mine_t], local.at[4]
        ),
    ]
    for copy in own:
        copy.start()

    ti, si = iota((T, T), 0), iota((T, T), 1)
    until = jnp.where(si <= ti, 1.0, 0.0)
    before = jnp.where(si < ti, 1.0, 0.0)
    jump = jnp.broadcast_to(jumps[...], (8, T))
    jump_in = nt(until, jump, HIGH)[:, 0:1]
    jump_ex = nt(before, jump, HIGH)[:, 0:1]
    jump_in_row = nt(jump, until, HIGH)[0:1, :]
    jump_ex_row = nt(jump, before, HIGH)[0:1, :]
    jump_all = jump_in_row[:, T - 1 : T]

    raw = query_in[...].astype(F32)
    queries = raw * jax.nn.sigmoid(raw)
    values = value_in[...]

    key_f = gate_gap[0:1, :] * jax.nn.sigmoid(-forget_fwd[...].astype(F32))
    log_f = jnp.log1p(-key_f)
    sum_f = nn(until, log_f, HIGH)
    all_f = sum_f[T - 1 : T, :]
    mid_f = all_f * 0.5
    scores = jnp.where(
        si <= ti,
        nt((queries * jnp.exp(sum_f - mid_f)).astype(BF16), (key_f * jnp.exp(mid_f - sum_f)).astype(BF16))
        * jnp.exp(jnp.minimum(jump_in - jump_in_row, 0.0)),
        0.0,
    )
    decay_f = jnp.exp(all_f + jump_all)
    state_f = tn(values, (key_f * jnp.exp((all_f - sum_f) + (jump_all - jump_in))).astype(BF16))
    reach_f = (queries * jnp.exp(sum_f + jump_in)).astype(BF16)

    key_b = gate_gap[1:2, :] * jax.nn.sigmoid(-forget_bwd[...].astype(F32))
    log_b = jnp.log1p(-key_b)
    sum_b = nn(before, log_b, HIGH)
    all_b = sum_b[T - 1 : T, :] + log_b[T - 1 : T, :]
    mid_b = all_b * 0.5
    scores = scores + jnp.where(
        si >= ti,
        nt((queries * jnp.exp(mid_b - sum_b)).astype(BF16), (key_b * jnp.exp(sum_b - mid_b)).astype(BF16))
        * jnp.exp(jnp.minimum(jump_ex_row - jump_ex, 0.0)),
        0.0,
    )
    decay_b = jnp.exp(all_b + jump_all)
    state_b = tn(values, (key_b * jnp.exp(sum_b + jump_ex)).astype(BF16))
    reach_b = (queries * jnp.exp((all_b - sum_b) + (jump_all - jump_ex))).astype(BF16)
    within = nn(scores.astype(BF16), values)

    i, j = iota((512, 256), 0), iota((512, 256), 1)
    r = i & 15
    place = onehot(((r < 8) & (j == (i >> 4) * 4 + (r & 3) + jnp.where(r < 4, 0, 128))))
    pieces = nn(place, jnp.concatenate([state_f.astype(BF16), state_b.astype(BF16)], axis=0))
    r = iota((512, W), 0) & 15
    for number, decay in ((8, decay_f), (10, decay_b)):
        high, low = split(decay)
        pieces = jnp.where(r == number, high.astype(F32), pieces)
        pieces = jnp.where(r == number + 1, low.astype(F32), pieces)
    states[...] = pieces.astype(BF16)

    pl.semaphore_wait(barrier, NSP + NTP - 2)

    def piece(ref):
        return lambda n: ref.at[pl.ds(pl.multiple_of(n * 16, 16), 16)]

    def slab(ref):
        return lambda n: ref.at[n, pl.ds(0, PAD)]

    there = Exchange("sp", NSP, piece(states), piece(got), zsend.at[0], zrecv.at[0])
    again = Exchange("sp", NSP, piece(answers), piece(carries), zsend.at[1], zrecv.at[1])
    shipped = Exchange("sp", NSP, slab(sent), slab(came), zsend.at[2], zrecv.at[2])
    returned = Exchange("sp", NSP, slab(outs), slab(back), zsend.at[3], zrecv.at[3])
    project = Exchange(
        "tp", NTP, lambda n: out_weight.at[:, pl.ds(pl.multiple_of(n * W, W), W)],
        lambda n: wo.at[n], tsend.at[0], trecv.at[0],
    )
    down = Exchange(
        "tp", NTP, lambda n: w_down.at[0, pl.ds(pl.multiple_of(n * 256, 256), 256)],
        lambda n: wd.at[:, pl.ds(pl.multiple_of(n * W, W), W)], tsend.at[1], trecv.at[1],
    )
    there.start()
    project.start()
    down.start()
    mine_s = pl.ds(pl.multiple_of(sp * 16, 16), 16)
    got[mine_s] = states[mine_s]

    ids = route_ids[...]
    weights = route_weights[...]
    lane = iota((T, W), 1)
    named = jnp.zeros((T, W), F32)
    weighted = jnp.zeros((T, W), F32)
    for n in range(4):
        hit = ids[:, n : n + 1] == lane
        named = named + jnp.where(hit, 1.0, 0.0)
        weighted = weighted + jnp.where(hit, weights[:, n : n + 1], 0.0)
    named16 = named.astype(BF16)
    rank16 = nn(before.astype(BF16), named16).astype(BF16)
    w_high, w_low = split(weighted)
    STEP = 384
    for c in range(SLOTS // STEP):
        slot, e = iota((STEP, W), 0) + c * STEP, iota((STEP, W), 1)
        owns = onehot((slot >= e * PAD) & (slot < e * PAD + PAD))
        number = nt(owns, jnp.broadcast_to(lax.broadcasted_iota(jnp.int32, (8, W), 1).astype(F32), (8, W)).astype(BF16))
        turn = (iota((STEP, 1), 0) + c * STEP).astype(F32) - PAD * number[:, 0:1]
        picked = (nt(owns, named16) > 0.5) & (nt(owns, rank16) == turn)
        disp[c * STEP : (c + 1) * STEP, :] = onehot(picked)

        slot, e = iota((W, STEP), 1) + c * STEP, iota((W, STEP), 0)
        owns = onehot((slot >= e * PAD) & (slot < e * PAD + PAD))
        number = nn(lax.broadcasted_iota(jnp.int32, (8, W), 1).astype(F32).astype(BF16), owns)
        turn = (iota((1, STEP), 1) + c * STEP).astype(F32) - PAD * number[0:1, :]
        picked = (nn(named16, owns) > 0.5) & (nn(rank16, owns) == turn)
        comb[0, :, c * STEP : (c + 1) * STEP] = jnp.where(picked, nn(w_high, owns), 0.0).astype(BF16)
        comb[1, :, c * STEP : (c + 1) * STEP] = jnp.where(picked, nn(w_low, owns), 0.0).astype(BF16)

    there.wait()

    def load(n):
        block = got[pl.ds(pl.multiple_of(n * 16, 16), 16)].astype(F32)
        return block[0:8], block[8:9] + block[9:10], block[10:11] + block[11:12]

    def forward(n, state):
        held, ahead, _ = load(n)
        scanned[pl.ds(pl.multiple_of(n * 8, 8), 8)] = state
        return state * ahead + held

    def backward(n, state):
        n = NSP - 1 - n
        held, _, behind = load(n)
        first = scanned[pl.ds(pl.multiple_of(n * 8, 8), 8)]
        both = jnp.where(iota((8, W), 0) < 4, first, state)
        answers[pl.ds(pl.multiple_of(n * 16, 16), 16)] = jnp.concatenate(
            [both, jnp.zeros((8, W), F32)], axis=0
        ).astype(BF16)
        return state * behind + held

    lax.fori_loop(0, NSP, forward, jnp.zeros((8, W), F32))
    lax.fori_loop(0, NSP, backward, jnp.zeros((8, W), F32))
    again.start()
    carries[mine_s] = answers[mine_s]
    again.wait()

    i, j = iota((W, 512), 0), iota((W, 512), 1)
    spot = (i >> 2) * 16 + (i & 3)
    enter_f = nn(onehot(j == spot), carries[...]).astype(BF16)
    enter_b = nn(onehot(j == spot + 4), carries[...]).astype(BF16)
    heads = within + nt(reach_f, enter_f) + nt(reach_b, enter_b)
    mean = jnp.mean(heads * heads, axis=-1, keepdims=True)
    gate = out_gate[...].astype(F32)
    gated = heads * lax.rsqrt(mean + EPS) * head_gain[...] * (gate * jax.nn.sigmoid(gate))
    gat[y, x] = gated.astype(BF16)
    heads_all = Gather(torus, gat, T, 0, gsend, grecv, 0)
    heads_all.run()
    own[0].wait()
    own[1].wait()
    project.wait()
    total = res[...].astype(F32)
    for n in range(NTP):
        total = total + nn(gat[n // 4, n % 4], wo[n])
    stream = total.astype(BF16)

    for c in range(SLOTS // STEP):
        sent[c * 8 : (c + 1) * 8] = (
            nn(disp[c * STEP : (c + 1) * STEP, :], stream).astype(BF16).reshape(8, PAD, W)
        )
    shipped.start()
    came[pl.ds(sp, 1)] = sent[pl.ds(sp, 1)]
    shipped.wait()
    i, j = iota((4 * CAP, 4 * PAD), 0), iota((4 * CAP, 4 * PAD), 1)
    pack = (j >= 0) & False
    for n in range(4):
        pack = pack | ((i >= n * CAP) & (i < (n + 1) * CAP) & (j == i + n * (PAD - CAP)))
    pack = onehot(pack)
    i, j = iota((4 * PAD, 4 * CAP), 0), iota((4 * PAD, 4 * CAP), 1)
    unpack = (j >= 0) & False
    for n in range(4):
        unpack = unpack | ((j >= n * CAP) & (j < (n + 1) * CAP) & (i == j + n * (PAD - CAP)))
    unpack = onehot(unpack)
    for g in range(8):
        rows[y, x, g * 4 * CAP : (g + 1) * 4 * CAP, :] = nn(
            pack, came[4 * g : 4 * g + 4].reshape(4 * PAD, W)
        ).astype(BF16)
    features = Gather(torus, rows, ROWS, 0, gsend, grecv, 1)
    features.run()

    own[2].wait()
    own[3].wait()
    own[4].wait()
    down.wait()

    @pl.loop(0, ROWS // TILE)
    def _(n):
        where = pl.ds(pl.multiple_of(n * TILE, TILE), TILE)
        squares = jnp.zeros((TILE, W), F32)
        for k in range(NTP):
            block = rows[k // 4, k % 4, where].astype(F32)
            squares = squares + block * block
            xs[:, k * W : (k + 1) * W] = (block * norm_gain[k : k + 1, :]).astype(BF16)
        scale = lax.rsqrt(jnp.sum(squares, axis=-1, keepdims=True) * (1.0 / (NTP * W)) + EPS)
        gates = jnp.minimum(nn(xs[...], wg[...]) * scale, LIMIT)
        ups = jnp.clip(nn(xs[...], wu[...]) * scale, -LIMIT, LIMIT)
        act[...] = (gates * jax.nn.sigmoid(ALPHA * gates) * (ups + 1.0)).astype(BF16)
        for k in range(4):
            wide_part = nn(act[...], wd[:, k * 512 : (k + 1) * 512]).astype(BF16)
            for l in range(4):
                part[k, l, where] = wide_part[:, l * W : (l + 1) * W]

    sums = Reduce(torus, part, ROWS, 0, wide, narrow, rsend, rrecv, 0)
    sums.run()
    for g in range(8):
        outs[4 * g : 4 * g + 4] = (
            nn(unpack, part[y, x, g * 4 * CAP : (g + 1) * 4 * CAP, :]).astype(BF16).reshape(4, PAD, W)
        )
    returned.start()
    back[pl.ds(sp, 1)] = outs[pl.ds(sp, 1)]
    returned.wait()
    answer = stream.astype(F32)
    for n in range(2):
        answer = answer + nn(comb[n], back[...].reshape(SLOTS, W))
    mixed[...] = answer.astype(BF16)
    heads_all.drain()
    features.drain()
    sums.drain()


def shards(
    residual, query_in, value_in, forget_fwd, forget_bwd, jumps, gate_gap, out_gate, head_gain,
    out_weight, norm_gain, route_ids, route_weights, w_gate, w_up, w_down,
):
    vmem = pl.BlockSpec(memory_space=pltpu.VMEM)
    hbm = pl.BlockSpec(memory_space=pl.ANY)
    dma = pltpu.SemaphoreType.DMA
    buf = pltpu.VMEM
    return pl.pallas_call(
        layer,
        out_shape=jax.ShapeDtypeStruct((T, W), BF16),
        in_specs=[hbm] + [vmem] * 8 + [hbm] + [vmem] * 3 + [hbm] * 3,
        out_specs=vmem,
        scratch_shapes=[
            buf((2048, 256), BF16), buf((2048, 256), BF16), buf((256, 2048), BF16),
            buf((NTP, W, W), BF16), buf((T, W), BF16),
            buf((512, W), BF16), buf((512, W), BF16), buf((256, W), F32), buf((512, W), BF16), buf((512, W), BF16),
            buf((4, 4, T, W), BF16), buf((SLOTS, T), BF16), buf((2, T, SLOTS), BF16),
            buf((NSP, PAD, W), BF16), buf((NSP, PAD, W), BF16), buf((4, 4, ROWS, W), BF16),
            buf((TILE, 2048), BF16), buf((TILE, 256), BF16), buf((4, 4, ROWS, W), BF16),
            buf((12, 4, ROWS // 4, W), BF16), buf((12, ROWS // 4, W), BF16),
            buf((NSP, PAD, W), BF16), buf((NSP, PAD, W), BF16),
            dma((5,)), dma((4, NSP)), dma((4, NSP)), dma((2, NTP)), dma((2, NTP)),
            dma((48,)), dma((48,)), dma((24,)), dma((24,)),
        ],
        compiler_params=pltpu.CompilerParams(
            collective_id=0, has_side_effects=True, vmem_limit_bytes=60 * 1024 * 1024
        ),
    )(
        residual, query_in, value_in, forget_fwd, forget_bwd, jumps, gate_gap, out_gate,
        head_gain.reshape(1, W), out_weight, norm_gain.reshape(NTP, W), route_ids, route_weights,
        w_gate, w_up, w_down,
    )


def solution(mesh):
    return jax.shard_map(
        shards,
        mesh=mesh,
        in_specs=(
            P("sp", None), P("sp", "tp"), P("sp", "tp"), P("sp", "tp"), P("sp", "tp"), P("tp", "sp"),
            P(None, "tp"), P("sp", "tp"), P("tp"), P("tp", None), P(), P("sp", None), P("sp", None),
            P("sp", None, "tp"), P("sp", None, "tp"), P("sp", None, "tp"),
        ),
        out_specs=P("sp", "tp"),
        check_vma=False,
    )
```

time: 398 us -> 162 us (0.41); the launches traced: 393 us -> 162 us
  waiting for transfers between devices: 190 us -> 0 us
  Pallas kernels: 0 us -> 158 us
  blocking collectives: 113 us -> 0 us
  starting transfers between devices: 22.7 us -> 0 us
  matrix products: 21.1 us -> 0 us
  local copies, waits for them, and re-layouts: 18.4 us -> 3.65 us
  between operations: 14.5 us -> 0.01 us
  other arithmetic: 12.4 us -> 0 us
    pallas_call x0 -> x1, Pallas kernels: none -> 158 us  [shards(): pl.pallas_call(layer, out_shape=jax.ShapeDtypeStruct((T, W), BF16), in_sp...]
    all_gather x2 -> x0, waiting for transfers between devices: 158 us -> none  [the longest x1 97.4 us: shards(): lax.all_gather(active, 'tp', axis=2, tiled=True)]
    all_gather x4 -> x0, blocking collectives: 65.5 us -> none  [all_in_one(): both, at, found = (lax.all_gather(jnp.concatenate(lines), axis), 0, {})]
    all_to_all x2 -> x0, blocking collectives: 47.9 us -> none  [the longest x1 42.3 us: shards(): lax.all_to_all(buffer, SP, split_axis=0, concat_axis=1, tiled=True)]
    all_to_all x3 -> x0, waiting for transfers between devices: 32.3 us -> none  [the longest x1 14.2 us: turned_blocks(): filled = lax.all_to_all(filled, axes[k], k, k, tiled=True)]
    all_to_all x3 -> x0, starting transfers between devices: 22.4 us -> none  [the longest x1 12 us: turned_blocks(): filled = lax.all_to_all(filled, axes[k], k, k, tiled=True)]
    dot_general x22 -> x0, matrix products: 21.1 us -> none  [the longest x1 6.53 us: shards(): jnp.einsum('esf,efd->esd', lax.all_gather(active, 'tp', axis=2, tiled=Tru...]
    gather x2 -> x0, local copies, waits for them, and re-layouts: 4.81 us -> none  [the longest x1 2.93 us: shards(): buffer = column_rows[slot_rows].reshape(EXPERTS, CAP, part_width)]
  transfers between devices with their start and end apart: 5 -> 0, of which waited for: 5 -> 0; matrix products, arithmetic and copies ran while one was open for 2% -> 0% of each run, Pallas kernels for 0% -> 0%
where the time goes in v1:
time: 162 us
  Pallas kernels  158 us (98%)
  local copies, waits for them, and re-layouts  3.65 us (2%)
    pallas_call x1, Pallas kernels, shards(): pl.pallas_call(layer, out_shape=jax.ShapeDtypeStruct((T, W), BF16), in_sp...  158 us
    unnamed x5, local copies, waits for them, and re-layouts  3.65 us

profile of v1, /device:TPU:1, one launch (start us, length us, event | category | flops | bytes accessed | tf_op | source)
XLA Modules:
  0.0 161.8 jit_solution(18374372190132663543)
XLA Ops:
  0.0 0.0 copy-start
  0.0 1.5 copy.17.route_ids
  1.5 0.0 copy-done
  1.5 0.8 copy.18.route_weights
  2.2 158.2 %shard_map.154 = bf16[192,128]{1,0:T(8,128)(2,1)} custom-call(bf16[192,2048]{1,0:T(8,128)(2,1)} %residual.1, bf16[192,128]{1,0:T(8,128)(2,1)} %query_in.1, bf16[192,128]{1,0:T(8,128)(2,1)} %value_in.1, bf16[192,128]{1,0:T(8,128)(2,1)} %forget_fwd.1, bf16[192,128]{1,0:T(8,128)(2,1)} %forget_bwd.1, f32[1,192]{1,0:T(1,128)} %jumps.1, f32[2,128]{1,0:T(2,128)} %gate_gap.1, ...), custom_call_target="tpu_custom_call" | custom-call | tf_op jit(solution)/shard_map/pallas_call | solution.py:504
  160.4 1.4 copy.20
Async XLA Ops:
  0.0 1.5 copy-start

commit v2 on v1

--- a/solution.py
+++ b/solution.py
@@ -17,7 +17,16 @@
 PAD = 48
 ROWS = NSP * CAP
 SLOTS = NSP * PAD
-TILE = 288
+SEND = 40
+CHUNKS = 4
+BLOCKS = NSP // CHUNKS
+TILE = BLOCKS * CAP
+PLAN = (
+    ("a0", 0), ("a0", 1), ("a1", 0), ("a1", 1), ("a0", 2), ("a2", 0), ("a2", 1), ("a1", 2), ("a3", 0), ("a0", 3),
+    ("a2", 2), ("a1", 3), ("a4", 0), ("r0", 0), ("a3", 2), ("a2", 3), ("r1", 0), ("a3", 3), ("a3", 1), ("a4", 2),
+    ("r0", 2), ("a4", 3), ("r0", 3), ("a4", 1), ("r1", 2), ("r1", 3), ("r0", 1), ("r2", 3), ("r1", 1), ("r3", 3),
+    ("r2", 2), ("r2", 1), ("r4", 3), ("r3", 2), ("r2", 0), ("r3", 1), ("r4", 2), ("r3", 0), ("r4", 1), ("r4", 0),
+)
 EPS = 1e-06
 LIMIT = 7.0
 ALPHA = 1.702
@@ -52,6 +61,10 @@
     return pltpu.make_async_remote_copy(
         src_ref=src, dst_ref=dst, send_sem=send, recv_sem=recv, device_id=device, device_id_type=MESH
     )
+
+
+def offset(n, size):
+    return (n + 1) // 2 if n % 2 else (size - n // 2) % size
 
 
 class Exchange:
@@ -60,22 +73,44 @@
         self.send, self.recv = send, recv
         self.me = lax.axis_index(axis)
 
-    def copy(self, d, to, slot):
+    def partners(self, n):
+        o = offset(n, self.size)
+        return lax.rem(self.me + o, self.size), lax.rem(self.me + self.size - o, self.size)
+
+    def out(self, n):
+        to, _ = self.partners(n)
         return remote(
-            self.source(to), self.target(slot), self.send.at[d], self.recv.at[d], {self.axis: to}
+            self.source(n, to), self.target(n, self.me), self.send.at[n], self.recv.at[n], {self.axis: to}
         )
 
-    def start(self):
-        @pl.loop(1, self.size)
-        def _(d):
-            to = lax.rem(self.me + d, self.size)
-            self.copy(d, to, self.me).start()
-
-    def wait(self):
-        @pl.loop(1, self.size)
-        def _(d):
-            origin = lax.rem(self.me - d + self.size, self.size)
-            self.copy(d, origin, origin).wait()
+    def into(self, n):
+        to, origin = self.partners(n)
+        return remote(
+            self.source(n, to), self.target(n, origin), self.send.at[n], self.recv.at[n], {self.axis: to}
+        )
+
+    def start(self, numbers):
+        for n in numbers:
+            self.out(n).start()
+
+    def wait(self, numbers):
+        for n in numbers:
+            self.into(n).wait_recv()
+
+    def drain(self):
+        for n in range(1, self.size):
+            self.out(n).wait_send()
+
+
+class Opposite(Exchange):
+    def partners(self, n):
+        to, origin = Exchange.partners(self, n)
+        return origin, to
+
+
+def quarters(rows):
+    first = -(-rows // 64) * 16
+    return (0, first), (first, rows // 2 - first)
 
 
 class Torus:
@@ -100,8 +135,8 @@
         self.send, self.recv, self.number = send, recv, number
 
     def view(self, half, stage, j, q):
-        piece = self.rows // 4
-        rows = pl.ds(self.base + half * (self.rows // 2) + q * piece, piece)
+        start, length = quarters(self.rows)[q]
+        rows = pl.ds(self.base + half * (self.rows // 2) + start, length)
         if (half == 0) == (stage == 0):
             return self.ref.at[self.t.y, j, rows] if stage == 0 else self.ref.at[:, j, rows]
         return self.ref.at[j, self.t.x, rows] if stage == 0 else self.ref.at[j, :, rows]
@@ -159,15 +194,16 @@
         return (half == 0) != (stage == 0)
 
     def view(self, half, stage, j, q):
-        piece = self.rows // 4
-        rows = pl.ds(self.base + half * (self.rows // 2) + q * piece, piece)
+        start, length = quarters(self.rows)[q]
+        rows = pl.ds(self.base + half * (self.rows // 2) + start, length)
         if self.along(half, stage):
             return self.ref.at[self.t.y, j, rows] if stage == 1 else self.ref.at[:, j, rows]
         return self.ref.at[j, self.t.x, rows] if stage == 1 else self.ref.at[j, :, rows]
 
     def slot(self, half, stage, k):
         n = (self.number * 2 + half) * 6 + k
-        return self.wide.at[n] if stage == 0 else self.narrow.at[n]
+        rows = pl.ds(0, quarters(self.rows)[k % 2][1])
+        return self.wide.at[n, :, rows] if stage == 0 else self.narrow.at[n, rows]
 
     def copy(self, half, stage, k):
         along = self.along(half, stage)
@@ -249,6 +285,8 @@
     torus = Torus()
     y, x = torus.y, torus.x
 
+    came[:, 32:PAD] = jnp.zeros((NSP, PAD - 32, W), BF16)
+    back[:, 32:PAD] = jnp.zeros((NSP, PAD - 32, W), BF16)
     barrier = pltpu.get_barrier_semaphore()
 
     @pl.loop(1, NSP)
@@ -291,12 +329,6 @@
     sum_f = nn(until, log_f, HIGH)
     all_f = sum_f[T - 1 : T, :]
     mid_f = all_f * 0.5
-    scores = jnp.where(
-        si <= ti,
-        nt((queries * jnp.exp(sum_f - mid_f)).astype(BF16), (key_f * jnp.exp(mid_f - sum_f)).astype(BF16))
-        * jnp.exp(jnp.minimum(jump_in - jump_in_row, 0.0)),
-        0.0,
-    )
     decay_f = jnp.exp(all_f + jump_all)
     state_f = tn(values, (key_f * jnp.exp((all_f - sum_f) + (jump_all - jump_in))).astype(BF16))
     reach_f = (queries * jnp.exp(sum_f + jump_in)).astype(BF16)
@@ -306,16 +338,9 @@
     sum_b = nn(before, log_b, HIGH)
     all_b = sum_b[T - 1 : T, :] + log_b[T - 1 : T, :]
     mid_b = all_b * 0.5
-    scores = scores + jnp.where(
-        si >= ti,
-        nt((queries * jnp.exp(mid_b - sum_b)).astype(BF16), (key_b * jnp.exp(sum_b - mid_b)).astype(BF16))
-        * jnp.exp(jnp.minimum(jump_ex_row - jump_ex, 0.0)),
-        0.0,
-    )
     decay_b = jnp.exp(all_b + jump_all)
     state_b = tn(values, (key_b * jnp.exp(sum_b + jump_ex)).astype(BF16))
     reach_b = (queries * jnp.exp((all_b - sum_b) + (jump_all - jump_ex))).astype(BF16)
-    within = nn(scores.astype(BF16), values)
 
     i, j = iota((512, 256), 0), iota((512, 256), 1)
     r = i & 15
@@ -330,39 +355,63 @@
 
     pl.semaphore_wait(barrier, NSP + NTP - 2)
 
-    def piece(ref):
-        return lambda n: ref.at[pl.ds(pl.multiple_of(n * 16, 16), 16)]
-
-    def slab(ref):
-        return lambda n: ref.at[n, pl.ds(0, PAD)]
-
-    there = Exchange("sp", NSP, piece(states), piece(got), zsend.at[0], zrecv.at[0])
-    again = Exchange("sp", NSP, piece(answers), piece(carries), zsend.at[1], zrecv.at[1])
-    shipped = Exchange("sp", NSP, slab(sent), slab(came), zsend.at[2], zrecv.at[2])
-    returned = Exchange("sp", NSP, slab(outs), slab(back), zsend.at[3], zrecv.at[3])
+    def part16(ref, n):
+        return ref.at[pl.ds(pl.multiple_of(n * 16, 16), 16)]
+
+    def slab(ref, n):
+        return ref.at[n, pl.ds(0, SEND)]
+
+    there = Exchange(
+        "sp", NSP, lambda n, to: part16(states, to), lambda n, me: part16(got, me), zsend.at[0], zrecv.at[0]
+    )
+    again = Exchange(
+        "sp", NSP, lambda n, to: part16(answers, to), lambda n, me: part16(carries, me), zsend.at[1], zrecv.at[1]
+    )
+    shipped = Exchange(
+        "sp", NSP, lambda n, to: slab(sent, to), lambda n, me: slab(came, n), zsend.at[2], zrecv.at[2]
+    )
+    returned = Opposite(
+        "sp", NSP, lambda n, to: slab(outs, n), lambda n, me: slab(back, me), zsend.at[3], zrecv.at[3]
+    )
     project = Exchange(
-        "tp", NTP, lambda n: out_weight.at[:, pl.ds(pl.multiple_of(n * W, W), W)],
-        lambda n: wo.at[n], tsend.at[0], trecv.at[0],
+        "tp", NTP, lambda n, to: out_weight.at[:, pl.ds(pl.multiple_of(to * W, W), W)],
+        lambda n, me: wo.at[me], tsend.at[0], trecv.at[0],
     )
     down = Exchange(
-        "tp", NTP, lambda n: w_down.at[0, pl.ds(pl.multiple_of(n * 256, 256), 256)],
-        lambda n: wd.at[:, pl.ds(pl.multiple_of(n * W, W), W)], tsend.at[1], trecv.at[1],
-    )
-    there.start()
-    project.start()
-    down.start()
+        "tp", NTP, lambda n, to: w_down.at[0, pl.ds(pl.multiple_of(to * 256, 256), 256)],
+        lambda n, me: wd.at[:, pl.ds(pl.multiple_of(me * W, W), W)], tsend.at[1], trecv.at[1],
+    )
+    far_first = tuple(range(NSP - 1, 0, -1))
+    there.start(far_first)
+    project.start(range(1, NTP))
+    down.start(range(1, NTP))
     mine_s = pl.ds(pl.multiple_of(sp * 16, 16), 16)
     got[mine_s] = states[mine_s]
 
+    scores = jnp.where(
+        si <= ti,
+        nt((queries * jnp.exp(sum_f - mid_f)).astype(BF16), (key_f * jnp.exp(mid_f - sum_f)).astype(BF16))
+        * jnp.exp(jnp.minimum(jump_in - jump_in_row, 0.0)),
+        0.0,
+    )
+    scores = scores + jnp.where(
+        si >= ti,
+        nt((queries * jnp.exp(mid_b - sum_b)).astype(BF16), (key_b * jnp.exp(sum_b - mid_b)).astype(BF16))
+        * jnp.exp(jnp.minimum(jump_ex_row - jump_ex, 0.0)),
+        0.0,
+    )
+    within = nn(scores.astype(BF16), values)
+
     ids = route_ids[...]
     weights = route_weights[...]
-    lane = iota((T, W), 1)
-    named = jnp.zeros((T, W), F32)
-    weighted = jnp.zeros((T, W), F32)
+    line = iota((W, T), 0)
+    named = jnp.zeros((W, T), F32)
+    weighted = jnp.zeros((W, T), F32)
     for n in range(4):
-        hit = ids[:, n : n + 1] == lane
+        hit = ids[n : n + 1, :] == line
         named = named + jnp.where(hit, 1.0, 0.0)
-        weighted = weighted + jnp.where(hit, weights[:, n : n + 1], 0.0)
+        weighted = weighted + jnp.where(hit, weights[n : n + 1, :], 0.0)
+    named, weighted = named.T, weighted.T
     named16 = named.astype(BF16)
     rank16 = nn(before.astype(BF16), named16).astype(BF16)
     w_high, w_low = split(weighted)
@@ -383,7 +432,7 @@
         comb[0, :, c * STEP : (c + 1) * STEP] = jnp.where(picked, nn(w_high, owns), 0.0).astype(BF16)
         comb[1, :, c * STEP : (c + 1) * STEP] = jnp.where(picked, nn(w_low, owns), 0.0).astype(BF16)
 
-    there.wait()
+    there.wait(range(1, NSP))
 
     def load(n):
         block = got[pl.ds(pl.multiple_of(n * 16, 16), 16)].astype(F32)
@@ -406,9 +455,9 @@
 
     lax.fori_loop(0, NSP, forward, jnp.zeros((8, W), F32))
     lax.fori_loop(0, NSP, backward, jnp.zeros((8, W), F32))
-    again.start()
+    again.start(far_first)
     carries[mine_s] = answers[mine_s]
-    again.wait()
+    again.wait(range(1, NSP))
 
     i, j = iota((W, 512), 0), iota((W, 512), 1)
     spot = (i >> 2) * 16 + (i & 3)
@@ -423,7 +472,7 @@
     heads_all.run()
     own[0].wait()
     own[1].wait()
-    project.wait()
+    project.wait(range(1, NTP))
     total = res[...].astype(F32)
     for n in range(NTP):
         total = total + nn(gat[n // 4, n % 4], wo[n])
@@ -433,9 +482,12 @@
         sent[c * 8 : (c + 1) * 8] = (
             nn(disp[c * STEP : (c + 1) * STEP, :], stream).astype(BF16).reshape(8, PAD, W)
         )
-    shipped.start()
-    came[pl.ds(sp, 1)] = sent[pl.ds(sp, 1)]
-    shipped.wait()
+    def blocks(c):
+        return [n for n in range(c * BLOCKS, (c + 1) * BLOCKS) if n]
+
+    for c in range(CHUNKS):
+        shipped.start(blocks(c))
+    came[0:1] = sent[pl.ds(sp, 1)]
     i, j = iota((4 * CAP, 4 * PAD), 0), iota((4 * CAP, 4 * PAD), 1)
     pack = (j >= 0) & False
     for n in range(4):
@@ -446,21 +498,22 @@
     for n in range(4):
         unpack = unpack | ((j >= n * CAP) & (j < (n + 1) * CAP) & (i == j + n * (PAD - CAP)))
     unpack = onehot(unpack)
-    for g in range(8):
-        rows[y, x, g * 4 * CAP : (g + 1) * 4 * CAP, :] = nn(
-            pack, came[4 * g : 4 * g + 4].reshape(4 * PAD, W)
-        ).astype(BF16)
-    features = Gather(torus, rows, ROWS, 0, gsend, grecv, 1)
-    features.run()
-
-    own[2].wait()
-    own[3].wait()
-    own[4].wait()
-    down.wait()
-
-    @pl.loop(0, ROWS // TILE)
-    def _(n):
-        where = pl.ds(pl.multiple_of(n * TILE, TILE), TILE)
+    features = [Gather(torus, rows, TILE, c * TILE, gsend, grecv, 1 + c) for c in range(CHUNKS)]
+    sums = [Reduce(torus, part, TILE, c * TILE, wide, narrow, rsend, rrecv, c) for c in range(CHUNKS)]
+
+    def each(step, *args):
+        for half in range(2):
+            step(half, *args)
+
+    def arrive(c):
+        shipped.wait(blocks(c))
+        for g in range(c * BLOCKS // 4, (c + 1) * BLOCKS // 4):
+            rows[y, x, g * 4 * CAP : (g + 1) * 4 * CAP, :] = nn(
+                pack, came[4 * g : 4 * g + 4].reshape(4 * PAD, W)
+            ).astype(BF16)
+
+    def compute(c):
+        where = slice(c * TILE, (c + 1) * TILE)
         squares = jnp.zeros((TILE, W), F32)
         for k in range(NTP):
             block = rows[k // 4, k % 4, where].astype(F32)
@@ -475,22 +528,71 @@
             for l in range(4):
                 part[k, l, where] = wide_part[:, l * W : (l + 1) * W]
 
-    sums = Reduce(torus, part, ROWS, 0, wide, narrow, rsend, rrecv, 0)
-    sums.run()
-    for g in range(8):
-        outs[4 * g : 4 * g + 4] = (
-            nn(unpack, part[y, x, g * 4 * CAP : (g + 1) * 4 * CAP, :]).astype(BF16).reshape(4, PAD, W)
-        )
-    returned.start()
-    back[pl.ds(sp, 1)] = outs[pl.ds(sp, 1)]
-    returned.wait()
+    def leave(c):
+        for g in range(c * BLOCKS // 4, (c + 1) * BLOCKS // 4):
+            outs[4 * g : 4 * g + 4] = (
+                nn(unpack, part[y, x, g * 4 * CAP : (g + 1) * 4 * CAP, :]).astype(BF16).reshape(4, PAD, W)
+            )
+        returned.start(blocks(c))
+
+    def a0(c):
+        arrive(c)
+        each(features[c].begin, 0)
+
+    def a1(c):
+        each(features[c].relay, 0)
+
+    def a2(c):
+        for half in range(2):
+            features[c].end(half, 0)
+            features[c].begin(half, 1)
+
+    def a3(c):
+        each(features[c].relay, 1)
+
+    def a4(c):
+        each(features[c].end, 1)
+
+    def r0(c):
+        if ("r0", c) == first:
+            own[2].wait()
+            own[3].wait()
+            own[4].wait()
+            down.wait(range(1, NTP))
+        compute(c)
+        each(sums[c].begin, 0)
+
+    def r1(c):
+        each(sums[c].relay, 0)
+
+    def r2(c):
+        for half in range(2):
+            sums[c].end(half, 0)
+            sums[c].begin(half, 1)
+
+    def r3(c):
+        each(sums[c].relay, 1)
+
+    def r4(c):
+        each(sums[c].end, 1)
+        leave(c)
+
+    steps = dict(a0=a0, a1=a1, a2=a2, a3=a3, a4=a4, r0=r0, r1=r1, r2=r2, r3=r3, r4=r4)
+    first = next(item for item in PLAN if item[0] == "r0")
+    for name, c in PLAN:
+        steps[name](c)
+    back[pl.ds(sp, 1)] = outs[0:1]
+    returned.wait(range(1, NSP))
     answer = stream.astype(F32)
     for n in range(2):
         answer = answer + nn(comb[n], back[...].reshape(SLOTS, W))
     mixed[...] = answer.astype(BF16)
     heads_all.drain()
-    features.drain()
-    sums.drain()
+    for c in range(CHUNKS):
+        features[c].drain()
+        sums[c].drain()
+    for each_one in (there, again, shipped, returned, project, down):
+        each_one.drain()
 
 
 def shards(
@@ -513,17 +615,17 @@
             buf((4, 4, T, W), BF16), buf((SLOTS, T), BF16), buf((2, T, SLOTS), BF16),
             buf((NSP, PAD, W), BF16), buf((NSP, PAD, W), BF16), buf((4, 4, ROWS, W), BF16),
             buf((TILE, 2048), BF16), buf((TILE, 256), BF16), buf((4, 4, ROWS, W), BF16),
-            buf((12, 4, ROWS // 4, W), BF16), buf((12, ROWS // 4, W), BF16),
+            buf((12 * CHUNKS, 4, 80, W), BF16), buf((12 * CHUNKS, 80, W), BF16),
             buf((NSP, PAD, W), BF16), buf((NSP, PAD, W), BF16),
             dma((5,)), dma((4, NSP)), dma((4, NSP)), dma((2, NTP)), dma((2, NTP)),
-            dma((48,)), dma((48,)), dma((24,)), dma((24,)),
+            dma((24 + 24 * CHUNKS,)), dma((24 + 24 * CHUNKS,)), dma((24 * CHUNKS,)), dma((24 * CHUNKS,)),
         ],
         compiler_params=pltpu.CompilerParams(
             collective_id=0, has_side_effects=True, vmem_limit_bytes=60 * 1024 * 1024
         ),
     )(
         residual, query_in, value_in, forget_fwd, forget_bwd, jumps, gate_gap, out_gate,
-        head_gain.reshape(1, W), out_weight, norm_gain.reshape(NTP, W), route_ids, route_weights,
+        head_gain.reshape(1, W), out_weight, norm_gain.reshape(NTP, W), route_ids.T, route_weights.T,
         w_gate, w_up, w_down,
     )
 

time: 162 us -> 139 us (0.86)
  Pallas kernels: 158 us -> 138 us
  local copies, waits for them, and re-layouts: 3.65 us -> 1.42 us
    pallas_call x1, Pallas kernels: 158 us -> 138 us  [shards(): pl.pallas_call(layer, out_shape=jax.ShapeDtypeStruct((T, W), BF16), in_sp...]
    unnamed x5 -> x1, local copies, waits for them, and re-layouts: 3.65 us -> 1.42 us
where the time goes in v2:
time: 139 us
  Pallas kernels  138 us (99%)
  local copies, waits for them, and re-layouts  1.42 us (1%)
    pallas_call x1, Pallas kernels, shards(): pl.pallas_call(layer, out_shape=jax.ShapeDtypeStruct((T, W), BF16), in_sp...  138 us

profile of v2, /device:TPU:1, one launch (start us, length us, event | category | flops | bytes accessed | tf_op | source)
XLA Modules:
  0.0 139.2 jit_solution(8889746565447533629)
XLA Ops:
  0.0 137.8 %shard_map.154 = bf16[192,128]{1,0:T(8,128)(2,1)} custom-call(bf16[192,2048]{1,0:T(8,128)(2,1)} %residual.1, bf16[192,128]{1,0:T(8,128)(2,1)} %query_in.1, bf16[192,128]{1,0:T(8,128)(2,1)} %value_in.1, bf16[192,128]{1,0:T(8,128)(2,1)} %forget_fwd.1, bf16[192,128]{1,0:T(8,128)(2,1)} %forget_bwd.1, f32[1,192]{1,0:T(1,128)} %jumps.1, f32[2,128]{1,0:T(2,128)} %gate_gap.1, ...), custom_call_target="tpu_custom_call" | custom-call | tf_op jit(solution)/shard_map/pallas_call | solution.py:606
  137.8 1.4 %copy.18 = bf16[192,128]{1,0:T(8,128)(2,1)} copy(bf16[192,128]{1,0:T(8,128)(2,1)} %shard_map.154) | data formatting | bytes 98304
